TPU v7x, 128 devices: a whole 4x4x4 slice. The times are simulated.
128 devices in a mesh: sp: 32 (over z, y, core), tp: 4 (over x).
Axes of the slice: x: 4, y: 4, z: 4, core: 2. Of those that a mesh axis runs over, the one named last changes fastest.
Arguments:
- tokens: bfloat16 [4, 2048, 1024], P(None, 'sp', 'tp'), may hold values from -6 to 6
- norm_gain: float32 [4, 1024], replicated, may hold values from 0.1 to 1.9
- val_weight: bfloat16 [4, 1024, 512], P(None, 'sp', 'tp'), may hold values from -0.1875 to 0.1875
- gate_weight: bfloat16 [4, 1024, 512], P(None, 'sp', 'tp'), may hold values from -0.1875 to 0.1875
- conv_taps: float32 [4, 31, 512], P(None, None, 'tp'), may hold values from -1 to 1
- conv_bias: float32 [4, 512], P(None, 'tp'), may hold values from -3 to 3
- ln_gain: float32 [4, 512], P(None, 'tp'), may hold values from 0.1 to 1.9
- ln_shift: float32 [4, 512], P(None, 'tp'), may hold values from -3 to 3
- out_weight: bfloat16 [4, 512, 1024], P(None, 'tp', 'sp'), may hold values from -0.25 to 0.25
Outputs:
- stream: bfloat16 [4, 2048, 1024], P(None, 'sp', 'tp')
All inputs are finite; a program needn't handle non-finite values.
Results may differ from a plain program's by a relative error of at most 0.02.
Values may be sent and summed in bfloat16 or wider, within the bound.
A program may use at most 64 MiB of HBM per device.

v0:
```python
from functools import partial
import jax
import jax.numpy as jnp
from jax import lax
from jax.sharding import PartitionSpec as P

LAYERS = 4
epsilon = 1e-06


def over_all(shard, axis, dim, absorb, state):
    everything = jax.tree.map(lambda a: lax.all_gather(a, axis, axis=dim, tiled=True), shard)
    return absorb(state, everything, jnp.int32(0))


def with_halo(shard, sides, width, wrap):
    for axis, dim in sides:
        size, length = (lax.axis_size(axis), shard.shape[dim])
        up = [(i, (i + 1) % size) for i in range(size if wrap else size - 1)]
        down = [(j, i) for i, j in up]
        last = lax.slice_in_dim(shard, length - width, length, axis=dim)
        initial = lax.slice_in_dim(shard, 0, width, axis=dim)
        before = lax.ppermute(last, axis, up)
        after = lax.ppermute(initial, axis, down)
        shard = jnp.concatenate([before, shard, after], axis=dim)
    return shard


def together(arrays, axis):
    ends = [0]
    for a in arrays:
        ends.append(ends[-1] + a.size)
    subtotal = lax.psum(jnp.concatenate([a.ravel() for a in arrays]), axis)
    return tuple((subtotal[b:e].reshape(a.shape) for a, b, e in zip(arrays, ends, ends[1:])))


def on_whole(shard, axis, dim, work):
    return work(lax.all_gather(shard, axis, axis=dim, tiled=True), jnp.int32(0))


def depthwise(padded, tap_weights, length):
    running = padded[:, 0:length] * tap_weights[0]
    for tap_idx in range(1, tap_weights.shape[0]):
        running = running + padded[:, tap_idx : tap_idx + length] * tap_weights[tap_idx]
    return running


def add_rows(left_rows, running, shard_piece, offset):
    columns = lax.dynamic_slice_in_dim(left_rows, offset, shard_piece.shape[0], 1)
    return running + jnp.dot(columns, shard_piece, preferred_element_type=jnp.float32)


def add_both(left_rows, totals, pieces, offset):
    return (
        add_rows(left_rows, totals[0], pieces[0], offset),
        add_rows(left_rows, totals[1], pieces[1], offset),
    )


def project_rows(left_rows, shard_piece, offset):
    return jnp.dot(left_rows, shard_piece, preferred_element_type=jnp.float32)


def shards(
    tokens, norm_gain, val_weight, gate_weight, conv_taps, conv_bias, ln_gain, ln_shift, out_weight
):
    stream = tokens
    num_seqs = tokens.shape[0]
    local_len = tokens.shape[1]
    chan_width = val_weight.shape[2]
    all_channels = chan_width * lax.axis_size("tp")
    half_width = conv_taps.shape[1] // 2
    for layer_idx in range(LAYERS):
        gathered = lax.all_gather(stream, "tp", axis=2, tiled=True)
        widened = gathered.astype(jnp.float32)
        scaled = widened * lax.rsqrt(jnp.mean(widened * widened, axis=-1, keepdims=True) + epsilon)
        normed = (scaled * norm_gain[layer_idx]).astype(jnp.bfloat16)
        tok_rows = normed.reshape(-1, normed.shape[2])
        zeroed = jnp.zeros((tok_rows.shape[0], chan_width), jnp.float32)
        values, gates = over_all(
            (val_weight[layer_idx], gate_weight[layer_idx]),
            "sp",
            0,
            partial(add_both, tok_rows),
            (zeroed, zeroed),
        )
        gated = (
            (values * jax.nn.sigmoid(gates))
            .astype(jnp.bfloat16)
            .reshape(num_seqs, local_len, chan_width)
        )
        padded = with_halo(gated, (("sp", 1),), half_width, False)
        convolved = (
            depthwise(padded.astype(jnp.float32), conv_taps[layer_idx], local_len)
            + conv_bias[layer_idx]
        )
        first_sum, second_sum = together(
            (jnp.sum(convolved, axis=-1), jnp.sum(convolved * convolved, axis=-1)), "tp"
        )
        mean_val = (first_sum / all_channels)[..., None]
        spread = (second_sum / all_channels)[..., None] - mean_val * mean_val
        centered = convolved - mean_val
        normalized = (
            centered * lax.rsqrt(spread + epsilon) * ln_gain[layer_idx] + ln_shift[layer_idx]
        )
        activated = jax.nn.silu(normalized).astype(jnp.bfloat16).reshape(-1, chan_width)
        partial_terms = on_whole(out_weight[layer_idx], "sp", 1, partial(project_rows, activated))
        full_width = partial_terms.shape[1]
        summed = lax.psum_scatter(
            partial_terms.reshape(num_seqs, local_len, full_width).astype(jnp.bfloat16),
            "tp",
            scatter_dimension=2,
            tiled=True,
        ).astype(jnp.float32)
        stream = (stream.astype(jnp.float32) + summed).astype(jnp.bfloat16)
    return stream


def solution(mesh):
    return jax.shard_map(
        shards,
        mesh=mesh,
        in_specs=(
            P(None, "sp", "tp"),
            P(),
            P(None, "sp", "tp"),
            P(None, "sp", "tp"),
            P(None, None, "tp"),
            P(None, "tp"),
            P(None, "tp"),
            P(None, "tp"),
            P(None, "tp", "sp"),
        ),
        out_specs=P(None, "sp", "tp"),
        check_vma=False,
    )
```

profile of v0, /device:TPU:0, one launch (start us, length us, event | category | flops | bytes accessed | tf_op | source)
XLA Modules:
  0.0 455.9 jit_solution(18299880186058381866)
XLA Ops:
  6.5 0.9 fusion.211
  7.4 13.5 %all_gather.48 = bf16[4,64,1024]{2,1,0:T(8,128)(2,1)S(1)} all-gather(bf16[4,64,256]{2,1,0:T(8,128)(2,1)} %param.9), channel_id=1, replica_groups=mesh['sp'=32,'tp'=4] {'tp'}, dimensions={2}, use_global_device_ids=true | all-gather | bytes 655360 | tf_op jit(solution)/shard_map/all_gather | solution.py:74
  21.1 0.6 copy-done.2
  21.6 26.5 %all-gather = bf16[1,1024,128]{2,1,0:T(8,128)(2,1)S(1)} all-gather(bf16[1,32,128]{2,1,0:T(8,128)(2,1)S(1)} %get-tuple-element.155), channel_id=2, replica_groups=mesh['sp'=32,'tp'=4] {'sp'}, dimensions={1}, use_global_device_ids=true | all-gather | bytes 270336 | tf_op jit(solution)/shard_map/all_gather | solution.py:12
  48.1 24.3 %all-gather.1 = bf16[1,1024,128]{2,1,0:T(8,128)(2,1)S(1)} all-gather(bf16[1,32,128]{2,1,0:T(8,128)(2,1)S(1)} %get-tuple-element.151), channel_id=3, replica_groups=mesh['sp'=32,'tp'=4] {'sp'}, dimensions={1}, use_global_device_ids=true | all-gather | bytes 270336 | tf_op jit(solution)/shard_map/all_gather | solution.py:12
  73.2 2.3 collective-permute-start
  75.5 1.3 collective-permute-start.1
  76.9 0.7 copy-done.5
  77.6 0.7 copy-done.6
  78.3 26.7 %all-gather.2 = bf16[1,128,1024]{1,2,0:T(8,128)(2,1)S(1)} all-gather(bf16[1,128,32]{1,2,0:T(8,128)(2,1)S(1)} %get-tuple-element.157), channel_id=4, replica_groups=mesh['sp'=32,'tp'=4] {'sp'}, dimensions={2}, use_global_device_ids=true | all-gather | bytes 270336 | tf_op jit(solution)/shard_map/all_gather | solution.py:38
  105.0 0.6 fusion.199
  105.7 10.7 %psum.28 = f32[512]{0:T(512)S(1)} all-reduce(f32[512]{0:T(512)S(1)} %pad_maximum_fusion), channel_id=1, replica_groups=mesh['sp'=32,'tp'=4] {'tp'}, use_global_device_ids=true, to_apply=%region_3.0 | all-reduce | flops 512 | bytes 4096 | tf_op jit(solution)/shard_map/psum | solution.py:33
  116.6 1.2 convolution_convert_fusion.3
  117.8 23.1 %all-gather.3 = bf16[1,1024,128]{2,1,0:T(8,128)(2,1)S(1)} all-gather(bf16[1,32,128]{2,1,0:T(8,128)(2,1)S(1)} %get-tuple-element.154), channel_id=5, replica_groups=mesh['sp'=32,'tp'=4] {'sp'}, dimensions={1}, use_global_device_ids=true | all-gather | bytes 270336 | tf_op jit(solution)/shard_map/all_gather | solution.py:12
  140.9 23.9 %all-gather.4 = bf16[1,1024,128]{2,1,0:T(8,128)(2,1)S(1)} all-gather(bf16[1,32,128]{2,1,0:T(8,128)(2,1)S(1)} %get-tuple-element.150), channel_id=6, replica_groups=mesh['sp'=32,'tp'=4] {'sp'}, dimensions={1}, use_global_device_ids=true | all-gather | bytes 270336 | tf_op jit(solution)/shard_map/all_gather | solution.py:12
  164.8 0.9 add_convert_fusion.3
  165.8 13.5 %all_gather.52 = bf16[4,64,1024]{2,1,0:T(8,128)(2,1)S(1)} all-gather(bf16[4,64,256]{2,1,0:T(8,128)(2,1)S(1)} %add_convert_fusion.3), channel_id=1, replica_groups=mesh['sp'=32,'tp'=4] {'tp'}, dimensions={2}, use_global_device_ids=true | all-gather | bytes 655360 | tf_op jit(solution)/shard_map/all_gather | solution.py:74
  180.0 0.3 fusion.17
  180.3 1.3 collective-permute-start.2
  181.6 1.3 collective-permute-start.3
  182.9 28.4 %all-gather.5 = bf16[1,128,1024]{1,2,0:T(8,128)(2,1)S(1)} all-gather(bf16[1,128,32]{1,2,0:T(8,128)(2,1)S(1)} %get-tuple-element.158), channel_id=7, replica_groups=mesh['sp'=32,'tp'=4] {'sp'}, dimensions={2}, use_global_device_ids=true | all-gather | bytes 270336 | tf_op jit(solution)/shard_map/all_gather | solution.py:38
  211.3 0.6 fusion.198
  212.0 7.7 %psum.29 = f32[512]{0:T(512)S(1)} all-reduce(f32[512]{0:T(512)S(1)} %pad_maximum_fusion.1), channel_id=1, replica_groups=mesh['sp'=32,'tp'=4] {'tp'}, use_global_device_ids=true, to_apply=%region_8.9 | all-reduce | flops 512 | bytes 4096 | tf_op jit(solution)/shard_map/psum | solution.py:33
  219.9 1.2 convolution_convert_fusion.2
  221.2 22.6 %all-gather.6 = bf16[1,1024,128]{2,1,0:T(8,128)(2,1)S(1)} all-gather(bf16[1,32,128]{2,1,0:T(8,128)(2,1)S(1)} %get-tuple-element.156), channel_id=8, replica_groups=mesh['sp'=32,'tp'=4] {'sp'}, dimensions={1}, use_global_device_ids=true | all-gather | bytes 270336 | tf_op jit(solution)/shard_map/all_gather | solution.py:12
  243.7 24.3 %all-gather.7 = bf16[1,1024,128]{2,1,0:T(8,128)(2,1)S(1)} all-gather(bf16[1,32,128]{2,1,0:T(8,128)(2,1)S(1)} %get-tuple-element.152), channel_id=9, replica_groups=mesh['sp'=32,'tp'=4] {'sp'}, dimensions={1}, use_global_device_ids=true | all-gather | bytes 270336 | tf_op jit(solution)/shard_map/all_gather | solution.py:12
  268.1 0.9 add_convert_fusion.2
  269.0 12.9 %all_gather.56 = bf16[4,64,1024]{2,1,0:T(8,128)(2,1)S(1)} all-gather(bf16[4,64,256]{2,1,0:T(8,128)(2,1)S(1)} %add_convert_fusion.2), channel_id=1, replica_groups=mesh['sp'=32,'tp'=4] {'tp'}, dimensions={2}, use_global_device_ids=true | all-gather | bytes 655360 | tf_op jit(solution)/shard_map/all_gather | solution.py:74
  282.6 0.3 fusion.18
  282.9 1.3 collective-permute-start.4
  284.2 1.3 collective-permute-start.5
  285.5 27.6 %all-gather.8 = bf16[1,128,1024]{1,2,0:T(8,128)(2,1)S(1)} all-gather(bf16[1,128,32]{1,2,0:T(8,128)(2,1)S(1)} %get-tuple-element.160), channel_id=10, replica_groups=mesh['sp'=32,'tp'=4] {'sp'}, dimensions={2}, use_global_device_ids=true | all-gather | bytes 270336 | tf_op jit(solution)/shard_map/all_gather | solution.py:38
  313.2 0.6 fusion.197
  313.9 9.9 %psum.30 = f32[512]{0:T(512)S(1)} all-reduce(f32[512]{0:T(512)S(1)} %pad_maximum_fusion.2), channel_id=1, replica_groups=mesh['sp'=32,'tp'=4] {'tp'}, use_global_device_ids=true, to_apply=%region_13.14 | all-reduce | flops 512 | bytes 4096 | tf_op jit(solution)/shard_map/psum | solution.py:33
  324.0 1.2 convolution_convert_fusion.1
  325.3 23.1 %all-gather.9 = bf16[1,1024,128]{2,1,0:T(8,128)(2,1)S(1)} all-gather(bf16[1,32,128]{2,1,0:T(8,128)(2,1)S(1)} %get-tuple-element.153), channel_id=11, replica_groups=mesh['sp'=32,'tp'=4] {'sp'}, dimensions={1}, use_global_device_ids=true | all-gather | bytes 270336 | tf_op jit(solution)/shard_map/all_gather | solution.py:12
  348.3 24.0 %all-gather.10 = bf16[1,1024,128]{2,1,0:T(8,128)(2,1)S(1)} all-gather(bf16[1,32,128]{2,1,0:T(8,128)(2,1)S(1)} %get-tuple-element.149), channel_id=12, replica_groups=mesh['sp'=32,'tp'=4] {'sp'}, dimensions={1}, use_global_device_ids=true | all-gather | bytes 270336 | tf_op jit(solution)/shard_map/all_gather | solution.py:12
  372.4 0.9 add_convert_fusion.1
  373.3 13.5 %all_gather.60 = bf16[4,64,1024]{2,1,0:T(8,128)(2,1)S(1)} all-gather(bf16[4,64,256]{2,1,0:T(8,128)(2,1)S(1)} %add_convert_fusion.1), channel_id=1, replica_groups=mesh['sp'=32,'tp'=4] {'tp'}, dimensions={2}, use_global_device_ids=true | all-gather | bytes 655360 | tf_op jit(solution)/shard_map/all_gather | solution.py:74
  387.5 0.3 fusion.19
  387.8 1.3 collective-permute-start.6
  389.1 1.3 collective-permute-start.7
  390.4 28.2 %all-gather.11 = bf16[1,128,1024]{1,2,0:T(8,128)(2,1)S(1)} all-gather(bf16[1,128,32]{1,2,0:T(8,128)(2,1)S(1)} %get-tuple-element.159), channel_id=13, replica_groups=mesh['sp'=32,'tp'=4] {'sp'}, dimensions={2}, use_global_device_ids=true | all-gather | bytes 270336 | tf_op jit(solution)/shard_map/all_gather | solution.py:38
  418.6 0.6 fusion.196
  419.4 7.7 %psum.31 = f32[512]{0:T(512)S(1)} all-reduce(f32[512]{0:T(512)S(1)} %pad_maximum_fusion.3), channel_id=1, replica_groups=mesh['sp'=32,'tp'=4] {'tp'}, use_global_device_ids=true, to_apply=%region_18.19 | all-reduce | flops 512 | bytes 4096 | tf_op jit(solution)/shard_map/psum | solution.py:33
  427.3 1.2 convolution_convert_fusion
  428.5 19.3 %reduce-scatter.11.cloned.1.call-done = bf16[4,64,256]{2,1,0:T(8,128)(2,1)} async-done(((bf16[4,64,1024]{2,1,0:T(8,128)(2,1)}), bf16[4,64,256]{2,1,0:T(8,128)(2,1)}) %reduce-scatter.11.cloned.1.call-update) | async-done | bytes 131088 | tf_op jit(solution)/shard_map/reduce_scatter | solution.py:109
  447.7 1.6 add_convert_fusion
  (97 shorter events, 5.0 us)
Async XLA Ops:
  6.5 158.3 %reduce-scatter.5.cloned.1.call-start = ((), (), s32[]{:S(2)}) async-start(), calls=%async_computation.4 | async-start | bytes 655360 | tf_op jit(solution)/shard_map/reduce_scatter | solution.py:109
  20.9 0.8 copy-start.2
  21.6 26.5 %copy-start.3 = (bf16[4,32,128]{2,1,0:T(8,128)(2,1)S(1)}, bf16[4,32,128]{2,1,0:T(8,128)(2,1)}, u32[]{:S(2)}) copy-start(bf16[4,32,128]{2,1,0:T(8,128)(2,1)} %param.12) | copy-start | bytes 98308
  73.2 3.6 copy-start.1
  73.2 4.3 copy-start.4
  73.2 31.7 %collective-permute-start = (bf16[4,15,128]{2,1,0:T(8,128)(2,1)S(1)}, bf16[4,15,128]{2,1,0:T(8,128)(2,1)S(1)}, u32[]{:S(2)}, u32[]{:S(2)}) collective-permute-start(bf16[4,15,128]{2,1,0:T(8,128)(2,1)S(1)} %get-tuple-element.23), channel_id=1, source_target_pairs={{0,4},{4,8},{8,12},{12,16},{16,20},{20,24},{24,28},{28,32},{32,36}... | collective-permute-start | bytes 46088 | tf_op jit(solution)/shard_map/ppermute | solution.py:23
  75.5 29.4 %collective-permute-start.1 = (bf16[4,15,128]{2,1,0:T(8,128)(2,1)S(1)}, bf16[4,15,128]{2,1,0:T(8,128)(2,1)S(1)}, u32[]{:S(2)}, u32[]{:S(2)}) collective-permute-start(bf16[4,15,128]{2,1,0:T(8,128)(2,1)S(1)} %get-tuple-element.24), channel_id=1, source_target_pairs={{4,0},{8,4},{12,8},{16,12},{20,16},{24,20},{28,24},{32,28},{36,32}... | collective-permute-start | bytes 46088 | tf_op jit(solution)/shard_map/ppermute | solution.py:24
  76.9 0.7 copy-start.5
  77.5 0.7 copy-start.6
  77.6 0.7 copy-start.7
  117.8 150.3 %reduce-scatter.7.cloned.1.call-start = ((), (), s32[]{:S(2)}) async-start(), calls=%async_computation.5 | async-start | bytes 655360 | tf_op jit(solution)/shard_map/reduce_scatter | solution.py:109
  140.9 23.9 %copy-start = (bf16[4,64,256]{2,1,0:T(8,128)(2,1)S(1)}, bf16[4,64,256]{2,1,0:T(8,128)(2,1)}, u32[]{:S(2)}) copy-start(bf16[4,64,256]{2,1,0:T(8,128)(2,1)} %param.9) | copy-start | bytes 393220
  180.3 31.0 %collective-permute-start.2 = (bf16[4,15,128]{2,1,0:T(8,128)(2,1)S(1)}, bf16[4,15,128]{2,1,0:T(8,128)(2,1)S(1)}, u32[]{:S(2)}, u32[]{:S(2)}) collective-permute-start(bf16[4,15,128]{2,1,0:T(8,128)(2,1)S(1)} %get-tuple-element.21), channel_id=1, source_target_pairs={{0,4},{4,8},{8,12},{12,16},{16,20},{20,24},{24,28},{28,32},{32,36}... | collective-permute-start | bytes 46088 | tf_op jit(solution)/shard_map/ppermute | solution.py:23
  181.6 29.7 %collective-permute-start.3 = (bf16[4,15,128]{2,1,0:T(8,128)(2,1)S(1)}, bf16[4,15,128]{2,1,0:T(8,128)(2,1)S(1)}, u32[]{:S(2)}, u32[]{:S(2)}) collective-permute-start(bf16[4,15,128]{2,1,0:T(8,128)(2,1)S(1)} %get-tuple-element.22), channel_id=1, source_target_pairs={{4,0},{8,4},{12,8},{16,12},{20,16},{24,20},{28,24},{32,28},{36,32}... | collective-permute-start | bytes 46088 | tf_op jit(solution)/shard_map/ppermute | solution.py:24
  221.1 151.2 %reduce-scatter.9.cloned.1.call-start = ((), (), s32[]{:S(2)}) async-start(), calls=%async_computation.6 | async-start | bytes 655360 | tf_op jit(solution)/shard_map/reduce_scatter | solution.py:109
  282.9 30.3 %collective-permute-start.4 = (bf16[4,15,128]{2,1,0:T(8,128)(2,1)S(1)}, bf16[4,15,128]{2,1,0:T(8,128)(2,1)S(1)}, u32[]{:S(2)}, u32[]{:S(2)}) collective-permute-start(bf16[4,15,128]{2,1,0:T(8,128)(2,1)S(1)} %get-tuple-element.19), channel_id=1, source_target_pairs={{0,4},{4,8},{8,12},{12,16},{16,20},{20,24},{24,28},{28,32},{32,36}... | collective-permute-start | bytes 46088 | tf_op jit(solution)/shard_map/ppermute | solution.py:23
  284.2 29.0 %collective-permute-start.5 = (bf16[4,15,128]{2,1,0:T(8,128)(2,1)S(1)}, bf16[4,15,128]{2,1,0:T(8,128)(2,1)S(1)}, u32[]{:S(2)}, u32[]{:S(2)}) collective-permute-start(bf16[4,15,128]{2,1,0:T(8,128)(2,1)S(1)} %get-tuple-element.20), channel_id=1, source_target_pairs={{4,0},{8,4},{12,8},{16,12},{20,16},{24,20},{28,24},{32,28},{36,32}... | collective-permute-start | bytes 46088 | tf_op jit(solution)/shard_map/ppermute | solution.py:24
  325.2 122.5 %reduce-scatter.11.cloned.1.call-start = ((), (), s32[]{:S(2)}) async-start(), calls=%async_computation.7 | async-start | bytes 655360 | tf_op jit(solution)/shard_map/reduce_scatter | solution.py:109
  387.8 30.8 %collective-permute-start.6 = (bf16[4,15,128]{2,1,0:T(8,128)(2,1)S(1)}, bf16[4,15,128]{2,1,0:T(8,128)(2,1)S(1)}, u32[]{:S(2)}, u32[]{:S(2)}) collective-permute-start(bf16[4,15,128]{2,1,0:T(8,128)(2,1)S(1)} %get-tuple-element.17), channel_id=1, source_target_pairs={{0,4},{4,8},{8,12},{12,16},{16,20},{20,24},{24,28},{28,32},{32,36}... | collective-permute-start | bytes 46088 | tf_op jit(solution)/shard_map/ppermute | solution.py:23
  389.1 29.5 %collective-permute-start.7 = (bf16[4,15,128]{2,1,0:T(8,128)(2,1)S(1)}, bf16[4,15,128]{2,1,0:T(8,128)(2,1)S(1)}, u32[]{:S(2)}, u32[]{:S(2)}) collective-permute-start(bf16[4,15,128]{2,1,0:T(8,128)(2,1)S(1)} %get-tuple-element.18), channel_id=1, source_target_pairs={{4,0},{8,4},{12,8},{16,12},{20,16},{24,20},{28,24},{32,28},{36,32}... | collective-permute-start | bytes 46088 | tf_op jit(solution)/shard_map/ppermute | solution.py:24
Sparse Core Ops, SparseCore 0:
  117.9 18.4 reduce-scatter.4
  221.2 19.1 reduce-scatter.6
  325.3 18.5 reduce-scatter.8
  428.6 19.1 reduce-scatter.10
where the time goes:
time: 457 us; the launch traced here: 456 us
  blocking collectives  392 us (86%)
  waiting for transfers between devices  19.4 us (4%)
  between operations  13.5 us (3%)
  starting transfers between devices  11.4 us (2%)
  other arithmetic  8.4 us (2%)
  matrix products  7 us (2%)
    all_gather x8, blocking collectives, over_all(): lax.all_gather(a, axis, axis=dim, tiled=True)  192 us
    all_gather x4, blocking collectives, on_whole(): return work(lax.all_gather(shard, axis, axis=dim, tiled=True), jnp.int32(0))  111 us
    all_gather x4, blocking collectives, shards(): gathered = lax.all_gather(stream, 'tp', axis=2, tiled=True)  53.4 us
    psum x4, blocking collectives, together(): subtotal = lax.psum(jnp.concatenate([a.ravel() for a in arrays]), axis)  36.1 us
    reduce_scatter x4, waiting for transfers between devices, shards(): lax.psum_scatter(partial_terms.reshape(num_seqs, local_len, full_width).a...  19.4 us
  transfers between devices with their start and end apart: 12, of which 1 were waited for; matrix products, arithmetic and copies ran while one was open for 0% of the time, Pallas kernels for 0%

commit v1 on v0

--- a/solution.py
+++ b/solution.py
@@ -6,6 +6,12 @@
 
 LAYERS = 4
 epsilon = 1e-06
+
+
+def in_order(parts, dim):
+    shape = list(parts.shape[1:])
+    shape[dim] *= parts.shape[0]
+    return jnp.moveaxis(parts, 0, dim).reshape(shape)
 
 
 def over_all(shard, axis, dim, absorb, state):
@@ -71,7 +77,19 @@
     all_channels = chan_width * lax.axis_size("tp")
     half_width = conv_taps.shape[1] // 2
     for layer_idx in range(LAYERS):
-        gathered = lax.all_gather(stream, "tp", axis=2, tiled=True)
+        count = lax.axis_size("tp")
+        pairs = [(i_2, (i_2 + 1) % count) for i_2 in range(count)]
+        back = [(b_2, a_2) for a_2, b_2 in pairs]
+        lower, upper = ([], [])
+        for step in range(count - 1):
+            if step % 2 == 0:
+                lower.append(lax.ppermute(lower[-1] if lower else stream, "tp", pairs))
+            else:
+                upper.append(lax.ppermute(upper[-1] if upper else stream, "tp", back))
+        parts = jnp.stack([*lower[::-1], stream, *upper])
+        shift = lax.axis_index("tp") - len(lower)
+        parts = parts[(jnp.arange(count) - shift) % count]
+        gathered = in_order(parts, 2)
         widened = gathered.astype(jnp.float32)
         scaled = widened * lax.rsqrt(jnp.mean(widened * widened, axis=-1, keepdims=True) + epsilon)
         normed = (scaled * norm_gain[layer_idx]).astype(jnp.bfloat16)

time: 457 us -> 512 us (1.12); the launches traced: 456 us -> 503 us
  waiting for transfers between devices: 19.4 us -> 83 us
  blocking collectives: 392 us -> 350 us
  starting transfers between devices: 11.4 us -> 27.9 us
  local copies, waits for them, and re-layouts: 4.25 us -> 12.3 us
    reduce_scatter x4, waiting for transfers between devices: 19.4 us -> 74.2 us  [shards(): lax.psum_scatter(partial_terms.reshape(num_seqs, local_len, full_width).a...]
    all_gather x4 -> x0, blocking collectives: 53.4 us -> none  [shards(): gathered = lax.all_gather(stream, 'tp', axis=2, tiled=True)]
    ppermute x0 -> x12, starting transfers between devices: none -> 13.5 us  [the longest x4 11.4 us: shards(): upper.append(lax.ppermute(upper[-1] if upper else stream, 'tp', back))]
    ppermute x0 -> x12, waiting for transfers between devices: none -> 8.76 us  [the longest x8 8.75 us: shards(): lower.append(lax.ppermute(lower[-1] if lower else stream, 'tp', pairs))]
    all_gather x8, blocking collectives: 192 us -> 200 us  [over_all(): lax.all_gather(a, axis, axis=dim, tiled=True)]
    psum x4, blocking collectives: 36.1 us -> 43.5 us  [together(): subtotal = lax.psum(jnp.concatenate([a.ravel() for a in arrays]), axis)]
  transfers between devices with their start and end apart: 12 -> 24, of which waited for: 1 -> 7; matrix products, arithmetic and copies ran while one was open for 0% -> 1% of each run, Pallas kernels for 0% -> 0%
where the time goes in v1:
time: 512 us; the launch traced here: 503 us
  blocking collectives  350 us (68%)
  waiting for transfers between devices  83 us (16%)
  starting transfers between devices  27.9 us (5%)
  between operations  13.9 us (3%)
  local copies, waits for them, and re-layouts  12.3 us (2%)
  other arithmetic  8.33 us (2%)
  matrix products  7.51 us (1%)
    all_gather x8, blocking collectives, over_all(): lax.all_gather(a, axis, axis=dim, tiled=True)  200 us
    all_gather x4, blocking collectives, on_whole(): return work(lax.all_gather(shard, axis, axis=dim, tiled=True), jnp.int32(0))  107 us
    reduce_scatter x4, waiting for transfers between devices, shards(): lax.psum_scatter(partial_terms.reshape(num_seqs, local_len, full_width).a...  74.2 us
    psum x4, blocking collectives, together(): subtotal = lax.psum(jnp.concatenate([a.ravel() for a in arrays]), axis)  43.5 us
    ppermute x4, starting transfers between devices, shards(): upper.append(lax.ppermute(upper[-1] if upper else stream, 'tp', back))  11.4 us
  transfers between devices with their start and end apart: 24, of which 7 were waited for; matrix products, arithmetic and copies ran while one was open for 1% of the time, Pallas kernels for 0%

profile of v1, /device:TPU:0, one launch (start us, length us, event | category | flops | bytes accessed | tf_op | source)
XLA Modules:
  0.0 503.1 jit_solution(13409084615116185455)
XLA Ops:
  6.5 1.6 collective-permute-start
  8.1 1.6 collective-permute-start.2
  9.8 0.9 slice_bitcast_fusion.101
  10.7 0.9 slice_bitcast_fusion.135
  11.5 0.8 slice_bitcast_fusion.134
  12.4 0.7 copy-done.3
  14.6 26.5 %all-gather = bf16[1,1024,128]{2,1,0:T(8,128)(2,1)S(1)} all-gather(bf16[1,32,128]{2,1,0:T(8,128)(2,1)S(1)} %get-tuple-element.153), channel_id=2, replica_groups=mesh['sp'=32,'tp'=4] {'sp'}, dimensions={1}, use_global_device_ids=true | all-gather | bytes 270336 | tf_op jit(solution)/shard_map/all_gather | solution.py:18
  41.5 24.4 %all-gather.1 = bf16[1,1024,128]{2,1,0:T(8,128)(2,1)S(1)} all-gather(bf16[1,32,128]{2,1,0:T(8,128)(2,1)S(1)} %get-tuple-element.151), channel_id=3, replica_groups=mesh['sp'=32,'tp'=4] {'sp'}, dimensions={1}, use_global_device_ids=true | all-gather | bytes 270336 | tf_op jit(solution)/shard_map/all_gather | solution.py:18
  68.6 2.3 collective-permute-start.3
  70.9 1.3 collective-permute-start.4
  72.2 26.7 %all-gather.2 = bf16[1,128,1024]{1,2,0:T(8,128)(2,1)S(1)} all-gather(bf16[1,128,32]{1,2,0:T(8,128)(2,1)S(1)} %get-tuple-element.157), channel_id=4, replica_groups=mesh['sp'=32,'tp'=4] {'sp'}, dimensions={2}, use_global_device_ids=true | all-gather | bytes 270336 | tf_op jit(solution)/shard_map/all_gather | solution.py:44
  99.6 10.7 %psum.28 = f32[512]{0:T(512)S(1)} all-reduce(f32[512]{0:T(512)S(1)} %pad_maximum_fusion.4), channel_id=1, replica_groups=mesh['sp'=32,'tp'=4] {'tp'}, use_global_device_ids=true, to_apply=%region_3.4 | all-reduce | flops 512 | bytes 4096 | tf_op jit(solution)/shard_map/psum | solution.py:39
  110.5 1.2 convolution_convert_fusion.3
  111.7 18.6 %reduce-scatter.5.cloned.1.call-done = bf16[4,64,256]{2,1,0:T(8,128)(2,1)} async-done(((bf16[4,64,1024]{2,1,0:T(8,128)(2,1)}), bf16[4,64,256]{2,1,0:T(8,128)(2,1)}) %reduce-scatter.5.cloned.1.call-update) | async-done | bytes 131088 | tf_op jit(solution)/shard_map/reduce_scatter | solution.py:127
  130.3 0.9 add_convert_fusion.3
  131.3 3.2 collective-permute-start.7
  134.6 2.9 collective-permute-done.5
  137.5 25.6 %all-gather.3 = bf16[1,1024,128]{2,1,0:T(8,128)(2,1)S(1)} all-gather(bf16[1,32,128]{2,1,0:T(8,128)(2,1)S(1)} %get-tuple-element.154), channel_id=5, replica_groups=mesh['sp'=32,'tp'=4] {'sp'}, dimensions={1}, use_global_device_ids=true | all-gather | bytes 270336 | tf_op jit(solution)/shard_map/all_gather | solution.py:18
  163.1 24.2 %all-gather.4 = bf16[1,1024,128]{2,1,0:T(8,128)(2,1)S(1)} all-gather(bf16[1,32,128]{2,1,0:T(8,128)(2,1)S(1)} %get-tuple-element.150), channel_id=6, replica_groups=mesh['sp'=32,'tp'=4] {'sp'}, dimensions={1}, use_global_device_ids=true | all-gather | bytes 270336 | tf_op jit(solution)/shard_map/all_gather | solution.py:18
  190.0 2.3 collective-permute-start.8
  192.2 1.3 collective-permute-start.9
  193.5 26.8 %all-gather.5 = bf16[1,128,1024]{1,2,0:T(8,128)(2,1)S(1)} all-gather(bf16[1,128,32]{1,2,0:T(8,128)(2,1)S(1)} %get-tuple-element.158), channel_id=7, replica_groups=mesh['sp'=32,'tp'=4] {'sp'}, dimensions={2}, use_global_device_ids=true | all-gather | bytes 270336 | tf_op jit(solution)/shard_map/all_gather | solution.py:44
  221.1 10.9 %psum.29 = f32[512]{0:T(512)S(1)} all-reduce(f32[512]{0:T(512)S(1)} %pad_maximum_fusion.5), channel_id=1, replica_groups=mesh['sp'=32,'tp'=4] {'tp'}, use_global_device_ids=true, to_apply=%region_8.9 | all-reduce | flops 512 | bytes 4096 | tf_op jit(solution)/shard_map/psum | solution.py:39
  232.2 1.2 convolution_convert_fusion.2
  233.4 18.5 %reduce-scatter.7.cloned.1.call-done = bf16[4,64,256]{2,1,0:T(8,128)(2,1)} async-done(((bf16[4,64,1024]{2,1,0:T(8,128)(2,1)}), bf16[4,64,256]{2,1,0:T(8,128)(2,1)}) %reduce-scatter.7.cloned.1.call-update) | async-done | bytes 131088 | tf_op jit(solution)/shard_map/reduce_scatter | solution.py:127
  252.0 0.9 add_convert_fusion.2
  253.0 3.3 collective-permute-start.12
  256.3 2.9 collective-permute-done.10
  259.2 25.1 %all-gather.6 = bf16[1,1024,128]{2,1,0:T(8,128)(2,1)S(1)} all-gather(bf16[1,32,128]{2,1,0:T(8,128)(2,1)S(1)} %get-tuple-element.156), channel_id=8, replica_groups=mesh['sp'=32,'tp'=4] {'sp'}, dimensions={1}, use_global_device_ids=true | all-gather | bytes 270336 | tf_op jit(solution)/shard_map/all_gather | solution.py:18
  284.3 24.4 %all-gather.7 = bf16[1,1024,128]{2,1,0:T(8,128)(2,1)S(1)} all-gather(bf16[1,32,128]{2,1,0:T(8,128)(2,1)S(1)} %get-tuple-element.152), channel_id=9, replica_groups=mesh['sp'=32,'tp'=4] {'sp'}, dimensions={1}, use_global_device_ids=true | all-gather | bytes 270336 | tf_op jit(solution)/shard_map/all_gather | solution.py:18
  311.3 2.3 collective-permute-start.13
  313.6 1.3 collective-permute-start.14
  314.9 26.8 %all-gather.8 = bf16[1,128,1024]{1,2,0:T(8,128)(2,1)S(1)} all-gather(bf16[1,128,32]{1,2,0:T(8,128)(2,1)S(1)} %get-tuple-element.160), channel_id=10, replica_groups=mesh['sp'=32,'tp'=4] {'sp'}, dimensions={2}, use_global_device_ids=true | all-gather | bytes 270336 | tf_op jit(solution)/shard_map/all_gather | solution.py:44
  342.4 10.9 %psum.30 = f32[512]{0:T(512)S(1)} all-reduce(f32[512]{0:T(512)S(1)} %pad_maximum_fusion.6), channel_id=1, replica_groups=mesh['sp'=32,'tp'=4] {'tp'}, use_global_device_ids=true, to_apply=%region_13.14 | all-reduce | flops 512 | bytes 4096 | tf_op jit(solution)/shard_map/psum | solution.py:39
  353.6 1.2 convolution_convert_fusion.1
  354.8 18.5 %reduce-scatter.9.cloned.1.call-done = bf16[4,64,256]{2,1,0:T(8,128)(2,1)} async-done(((bf16[4,64,1024]{2,1,0:T(8,128)(2,1)}), bf16[4,64,256]{2,1,0:T(8,128)(2,1)}) %reduce-scatter.9.cloned.1.call-update) | async-done | bytes 131088 | tf_op jit(solution)/shard_map/reduce_scatter | solution.py:127
  373.3 0.9 add_convert_fusion.1
  374.3 3.2 collective-permute-start.17
  377.6 2.9 collective-permute-done.15
  380.5 25.1 %all-gather.9 = bf16[1,1024,128]{2,1,0:T(8,128)(2,1)S(1)} all-gather(bf16[1,32,128]{2,1,0:T(8,128)(2,1)S(1)} %get-tuple-element.155), channel_id=11, replica_groups=mesh['sp'=32,'tp'=4] {'sp'}, dimensions={1}, use_global_device_ids=true | all-gather | bytes 270336 | tf_op jit(solution)/shard_map/all_gather | solution.py:18
  405.6 24.4 %all-gather.10 = bf16[1,1024,128]{2,1,0:T(8,128)(2,1)S(1)} all-gather(bf16[1,32,128]{2,1,0:T(8,128)(2,1)S(1)} %get-tuple-element.149), channel_id=12, replica_groups=mesh['sp'=32,'tp'=4] {'sp'}, dimensions={1}, use_global_device_ids=true | all-gather | bytes 270336 | tf_op jit(solution)/shard_map/all_gather | solution.py:18
  432.7 2.3 collective-permute-start.18
  435.0 1.3 collective-permute-start.19
  436.3 26.8 %all-gather.11 = bf16[1,128,1024]{1,2,0:T(8,128)(2,1)S(1)} all-gather(bf16[1,128,32]{1,2,0:T(8,128)(2,1)S(1)} %get-tuple-element.159), channel_id=13, replica_groups=mesh['sp'=32,'tp'=4] {'sp'}, dimensions={2}, use_global_device_ids=true | all-gather | bytes 270336 | tf_op jit(solution)/shard_map/all_gather | solution.py:44
  463.8 10.9 %psum.31 = f32[512]{0:T(512)S(1)} all-reduce(f32[512]{0:T(512)S(1)} %pad_maximum_fusion.7), channel_id=1, replica_groups=mesh['sp'=32,'tp'=4] {'tp'}, use_global_device_ids=true, to_apply=%region_18.19 | all-reduce | flops 512 | bytes 4096 | tf_op jit(solution)/shard_map/psum | solution.py:39
  475.0 1.2 convolution_convert_fusion
  476.1 18.6 %reduce-scatter.11.cloned.1.call-done = bf16[4,64,256]{2,1,0:T(8,128)(2,1)} async-done(((bf16[4,64,1024]{2,1,0:T(8,128)(2,1)}), bf16[4,64,256]{2,1,0:T(8,128)(2,1)}) %reduce-scatter.11.cloned.1.call-update) | async-done | bytes 131088 | tf_op jit(solution)/shard_map/reduce_scatter | solution.py:127
  494.7 1.6 add_convert_fusion
  (141 shorter events, 16.6 us)
Async XLA Ops:
  6.5 123.8 %reduce-scatter.5.cloned.1.call-start = ((), (), s32[]{:S(2)}) async-start(), calls=%async_computation.4 | async-start | bytes 655360 | tf_op jit(solution)/shard_map/reduce_scatter | solution.py:127
  6.5 34.6 %collective-permute-start = (bf16[4,64,256]{2,1,0:T(8,128)(2,1)}, bf16[4,64,256]{2,1,0:T(8,128)(2,1)S(1)}, u32[]{:S(2)}, u32[]{:S(2)}) collective-permute-start(bf16[4,64,256]{2,1,0:T(8,128)(2,1)} %param.9), channel_id=1, source_target_pairs={{0,1},{1,2},{2,3},{3,0},{4,5},{5,6},{6,7},{7,4},{8,9},{9,10},{10,1... | collective-permute-start | bytes 393224 | tf_op jit(solution)/shard_map/ppermute | solution.py:86
  8.1 57.7 %collective-permute-start.2 = (bf16[4,64,256]{2,1,0:T(8,128)(2,1)}, bf16[4,64,256]{2,1,0:T(8,128)(2,1)S(1)}, u32[]{:S(2)}, u32[]{:S(2)}) collective-permute-start(bf16[4,64,256]{2,1,0:T(8,128)(2,1)} %param.9), channel_id=1, source_target_pairs={{1,0},{2,1},{3,2},{0,3},{5,4},{6,5},{7,6},{4,7},{9,8},{10,9},{11,1... | collective-permute-start | bytes 393224 | tf_op jit(solution)/shard_map/ppermute | solution.py:88
  9.8 2.6 copy-start.5
  10.6 1.7 copy-start.2
  12.4 0.8 copy-start.3
  13.2 0.7 copy-start.6
  13.2 0.8 copy-start.4
  13.9 0.7 copy-start.7
  13.9 0.7 copy-start.8
  41.1 24.8 %collective-permute-start.1 = (bf16[4,64,256]{2,1,0:T(8,128)(2,1)S(1)}, bf16[4,64,256]{2,1,0:T(8,128)(2,1)S(1)}, u32[]{:S(2)}, u32[]{:S(2)}) collective-permute-start(bf16[4,64,256]{2,1,0:T(8,128)(2,1)S(1)} %collective-permute-done), channel_id=1, source_target_pairs={{0,1},{1,2},{2,3},{3,0},{4,5},{5,6},{6,7},{7,4},{8,9},{9,10},{10,1... | collective-permute-start | bytes 393224 | tf_op jit(solution)/shard_map/ppermute | solution.py:86
  41.5 24.4 %copy-start = (bf16[4,64,256]{2,1,0:T(8,128)(2,1)S(1)}, bf16[4,64,256]{2,1,0:T(8,128)(2,1)}, u32[]{:S(2)}) copy-start(bf16[4,64,256]{2,1,0:T(8,128)(2,1)} %param.9) | copy-start | bytes 393220
  68.6 30.3 %collective-permute-start.3 = (bf16[4,15,128]{2,1,0:T(8,128)(2,1)S(1)}, bf16[4,15,128]{2,1,0:T(8,128)(2,1)S(1)}, u32[]{:S(2)}, u32[]{:S(2)}) collective-permute-start(bf16[4,15,128]{2,1,0:T(8,128)(2,1)S(1)} %get-tuple-element.23), channel_id=1, source_target_pairs={{0,4},{4,8},{8,12},{12,16},{16,20},{20,24},{24,28},{28,32},{32,36}... | collective-permute-start | bytes 46088 | tf_op jit(solution)/shard_map/ppermute | solution.py:29
  70.9 28.0 %collective-permute-start.4 = (bf16[4,15,128]{2,1,0:T(8,128)(2,1)S(1)}, bf16[4,15,128]{2,1,0:T(8,128)(2,1)S(1)}, u32[]{:S(2)}, u32[]{:S(2)}) collective-permute-start(bf16[4,15,128]{2,1,0:T(8,128)(2,1)S(1)} %get-tuple-element.24), channel_id=1, source_target_pairs={{4,0},{8,4},{12,8},{16,12},{20,16},{24,20},{28,24},{32,28},{36,32}... | collective-permute-start | bytes 46088 | tf_op jit(solution)/shard_map/ppermute | solution.py:30
  111.7 25.8 %copy-start.1 = (f32[4,31,128]{2,0,1:T(4,128)S(1)}, f32[4,31,128]{2,0,1:T(4,128)}, u32[]{:S(2)}) copy-start(f32[4,31,128]{2,0,1:T(4,128)} %param.13) | copy-start | bytes 190468
  111.7 140.3 %reduce-scatter.7.cloned.1.call-start = ((), (), s32[]{:S(2)}) async-start(), calls=%async_computation.5 | async-start | bytes 655360 | tf_op jit(solution)/shard_map/reduce_scatter | solution.py:127
  131.2 6.2 %collective-permute-start.5 = (bf16[4,64,256]{2,1,0:T(8,128)(2,1)S(1)}, bf16[4,64,256]{2,1,0:T(8,128)(2,1)S(1)}, u32[]{:S(2)}, u32[]{:S(2)}) collective-permute-start(bf16[4,64,256]{2,1,0:T(8,128)(2,1)S(1)} %add_convert_fusion.3), channel_id=1, source_target_pairs={{0,1},{1,2},{2,3},{3,0},{4,5},{5,6},{6,7},{7,4},{8,9},{9,10},{10,1... | collective-permute-start | bytes 393224 | tf_op jit(solution)/shard_map/ppermute | solution.py:86
  131.3 56.0 %collective-permute-start.7 = (bf16[4,64,256]{2,1,0:T(8,128)(2,1)S(1)}, bf16[4,64,256]{2,1,0:T(8,128)(2,1)S(1)}, u32[]{:S(2)}, u32[]{:S(2)}) collective-permute-start(bf16[4,64,256]{2,1,0:T(8,128)(2,1)S(1)} %add_convert_fusion.3), channel_id=1, source_target_pairs={{1,0},{2,1},{3,2},{0,3},{5,4},{6,5},{7,6},{4,7},{9,8},{10,9},{11,1... | collective-permute-start | bytes 393224 | tf_op jit(solution)/shard_map/ppermute | solution.py:88
  137.5 49.8 %collective-permute-start.6 = (bf16[4,64,256]{2,1,0:T(8,128)(2,1)S(1)}, bf16[4,64,256]{2,1,0:T(8,128)(2,1)S(1)}, u32[]{:S(2)}, u32[]{:S(2)}) collective-permute-start(bf16[4,64,256]{2,1,0:T(8,128)(2,1)S(1)} %collective-permute-done.5), channel_id=1, source_target_pairs={{0,1},{1,2},{2,3},{3,0},{4,5},{5,6},{6,7},{7,4},{8,9},{9,10},{10,1... | collective-permute-start | bytes 393224 | tf_op jit(solution)/shard_map/ppermute | solution.py:86
  190.0 30.3 %collective-permute-start.8 = (bf16[4,15,128]{2,1,0:T(8,128)(2,1)S(1)}, bf16[4,15,128]{2,1,0:T(8,128)(2,1)S(1)}, u32[]{:S(2)}, u32[]{:S(2)}) collective-permute-start(bf16[4,15,128]{2,1,0:T(8,128)(2,1)S(1)} %get-tuple-element.21), channel_id=1, source_target_pairs={{0,4},{4,8},{8,12},{12,16},{16,20},{20,24},{24,28},{28,32},{32,36}... | collective-permute-start | bytes 46088 | tf_op jit(solution)/shard_map/ppermute | solution.py:29
  192.2 28.1 %collective-permute-start.9 = (bf16[4,15,128]{2,1,0:T(8,128)(2,1)S(1)}, bf16[4,15,128]{2,1,0:T(8,128)(2,1)S(1)}, u32[]{:S(2)}, u32[]{:S(2)}) collective-permute-start(bf16[4,15,128]{2,1,0:T(8,128)(2,1)S(1)} %get-tuple-element.22), channel_id=1, source_target_pairs={{4,0},{8,4},{12,8},{16,12},{20,16},{24,20},{28,24},{32,28},{36,32}... | collective-permute-start | bytes 46088 | tf_op jit(solution)/shard_map/ppermute | solution.py:30
  233.4 139.9 %reduce-scatter.9.cloned.1.call-start = ((), (), s32[]{:S(2)}) async-start(), calls=%async_computation.6 | async-start | bytes 655360 | tf_op jit(solution)/shard_map/reduce_scatter | solution.py:127
  252.9 6.2 %collective-permute-start.10 = (bf16[4,64,256]{2,1,0:T(8,128)(2,1)S(1)}, bf16[4,64,256]{2,1,0:T(8,128)(2,1)S(1)}, u32[]{:S(2)}, u32[]{:S(2)}) collective-permute-start(bf16[4,64,256]{2,1,0:T(8,128)(2,1)S(1)} %add_convert_fusion.2), channel_id=1, source_target_pairs={{0,1},{1,2},{2,3},{3,0},{4,5},{5,6},{6,7},{7,4},{8,9},{9,10},{10,1... | collective-permute-start | bytes 393224 | tf_op jit(solution)/shard_map/ppermute | solution.py:86
  253.0 55.6 %collective-permute-start.12 = (bf16[4,64,256]{2,1,0:T(8,128)(2,1)S(1)}, bf16[4,64,256]{2,1,0:T(8,128)(2,1)S(1)}, u32[]{:S(2)}, u32[]{:S(2)}) collective-permute-start(bf16[4,64,256]{2,1,0:T(8,128)(2,1)S(1)} %add_convert_fusion.2), channel_id=1, source_target_pairs={{1,0},{2,1},{3,2},{0,3},{5,4},{6,5},{7,6},{4,7},{9,8},{10,9},{11,1... | collective-permute-start | bytes 393224 | tf_op jit(solution)/shard_map/ppermute | solution.py:88
  259.1 49.5 %collective-permute-start.11 = (bf16[4,64,256]{2,1,0:T(8,128)(2,1)S(1)}, bf16[4,64,256]{2,1,0:T(8,128)(2,1)S(1)}, u32[]{:S(2)}, u32[]{:S(2)}) collective-permute-start(bf16[4,64,256]{2,1,0:T(8,128)(2,1)S(1)} %collective-permute-done.10), channel_id=1, source_target_pairs={{0,1},{1,2},{2,3},{3,0},{4,5},{5,6},{6,7},{7,4},{8,9},{9,10},{10,1... | collective-permute-start | bytes 393224 | tf_op jit(solution)/shard_map/ppermute | solution.py:86
  311.3 30.3 %collective-permute-start.13 = (bf16[4,15,128]{2,1,0:T(8,128)(2,1)S(1)}, bf16[4,15,128]{2,1,0:T(8,128)(2,1)S(1)}, u32[]{:S(2)}, u32[]{:S(2)}) collective-permute-start(bf16[4,15,128]{2,1,0:T(8,128)(2,1)S(1)} %get-tuple-element.19), channel_id=1, source_target_pairs={{0,4},{4,8},{8,12},{12,16},{16,20},{20,24},{24,28},{28,32},{32,36}... | collective-permute-start | bytes 46088 | tf_op jit(solution)/shard_map/ppermute | solution.py:29
  313.6 28.1 %collective-permute-start.14 = (bf16[4,15,128]{2,1,0:T(8,128)(2,1)S(1)}, bf16[4,15,128]{2,1,0:T(8,128)(2,1)S(1)}, u32[]{:S(2)}, u32[]{:S(2)}) collective-permute-start(bf16[4,15,128]{2,1,0:T(8,128)(2,1)S(1)} %get-tuple-element.20), channel_id=1, source_target_pairs={{4,0},{8,4},{12,8},{16,12},{20,16},{24,20},{28,24},{32,28},{36,32}... | collective-permute-start | bytes 46088 | tf_op jit(solution)/shard_map/ppermute | solution.py:30
  354.8 140.0 %reduce-scatter.11.cloned.1.call-start = ((), (), s32[]{:S(2)}) async-start(), calls=%async_computation.7 | async-start | bytes 655360 | tf_op jit(solution)/shard_map/reduce_scatter | solution.py:127
  374.3 6.2 %collective-permute-start.15 = (bf16[4,64,256]{2,1,0:T(8,128)(2,1)S(1)}, bf16[4,64,256]{2,1,0:T(8,128)(2,1)S(1)}, u32[]{:S(2)}, u32[]{:S(2)}) collective-permute-start(bf16[4,64,256]{2,1,0:T(8,128)(2,1)S(1)} %add_convert_fusion.1), channel_id=1, source_target_pairs={{0,1},{1,2},{2,3},{3,0},{4,5},{5,6},{6,7},{7,4},{8,9},{9,10},{10,1... | collective-permute-start | bytes 393224 | tf_op jit(solution)/shard_map/ppermute | solution.py:86
  374.3 55.7 %collective-permute-start.17 = (bf16[4,64,256]{2,1,0:T(8,128)(2,1)S(1)}, bf16[4,64,256]{2,1,0:T(8,128)(2,1)S(1)}, u32[]{:S(2)}, u32[]{:S(2)}) collective-permute-start(bf16[4,64,256]{2,1,0:T(8,128)(2,1)S(1)} %add_convert_fusion.1), channel_id=1, source_target_pairs={{1,0},{2,1},{3,2},{0,3},{5,4},{6,5},{7,6},{4,7},{9,8},{10,9},{11,1... | collective-permute-start | bytes 393224 | tf_op jit(solution)/shard_map/ppermute | solution.py:88
  380.5 49.5 %collective-permute-start.16 = (bf16[4,64,256]{2,1,0:T(8,128)(2,1)S(1)}, bf16[4,64,256]{2,1,0:T(8,128)(2,1)S(1)}, u32[]{:S(2)}, u32[]{:S(2)}) collective-permute-start(bf16[4,64,256]{2,1,0:T(8,128)(2,1)S(1)} %collective-permute-done.15), channel_id=1, source_target_pairs={{0,1},{1,2},{2,3},{3,0},{4,5},{5,6},{6,7},{7,4},{8,9},{9,10},{10,1... | collective-permute-start | bytes 393224 | tf_op jit(solution)/shard_map/ppermute | solution.py:86
  432.7 30.3 %collective-permute-start.18 = (bf16[4,15,128]{2,1,0:T(8,128)(2,1)S(1)}, bf16[4,15,128]{2,1,0:T(8,128)(2,1)S(1)}, u32[]{:S(2)}, u32[]{:S(2)}) collective-permute-start(bf16[4,15,128]{2,1,0:T(8,128)(2,1)S(1)} %get-tuple-element.17), channel_id=1, source_target_pairs={{0,4},{4,8},{8,12},{12,16},{16,20},{20,24},{24,28},{28,32},{32,36}... | collective-permute-start | bytes 46088 | tf_op jit(solution)/shard_map/ppermute | solution.py:29
  435.0 28.1 %collective-permute-start.19 = (bf16[4,15,128]{2,1,0:T(8,128)(2,1)S(1)}, bf16[4,15,128]{2,1,0:T(8,128)(2,1)S(1)}, u32[]{:S(2)}, u32[]{:S(2)}) collective-permute-start(bf16[4,15,128]{2,1,0:T(8,128)(2,1)S(1)} %get-tuple-element.18), channel_id=1, source_target_pairs={{4,0},{8,4},{12,8},{16,12},{20,16},{24,20},{28,24},{32,28},{36,32}... | collective-permute-start | bytes 46088 | tf_op jit(solution)/shard_map/ppermute | solution.py:30
Sparse Core Ops, SparseCore 0:
  111.8 18.4 reduce-scatter.4
  233.5 18.3 reduce-scatter.6
  354.9 18.3 reduce-scatter.8
  476.3 18.3 reduce-scatter.10
